TPU v7x, 32 devices: a whole 2x2x4 slice. The times are simulated.
32 devices in a mesh: ep: 8 (over z, y), tp: 4 (over x, core).
Axes of the slice: x: 2, y: 2, z: 4, core: 2. Of those that a mesh axis runs over, the one named last changes fastest.
Arguments:
- query_rows: bfloat16 [4096, 2048], P('ep', 'tp'), may hold values from -6 to 6
- key_rows: bfloat16 [4096, 512], P('ep', 'tp'), may hold values from -6 to 6
- value_rows: bfloat16 [4096, 512], P('ep', 'tp'), may hold values from -6 to 6
- query_gain: float32 [64], replicated, may hold values from 0.2 to 4.5
- key_gain: float32 [64], replicated, may hold values from 0.2 to 4.5
- sink_logit: float32 [32], P('tp'), may hold values from 2 to 6
- out_weight: bfloat16 [2048, 2048], P('tp'), may hold values from -0.125 to 0.125
- tokens: bfloat16 [4096, 2048], P('ep'), may hold values from -6 to 6
- norm_gain: float32 [2048], replicated, may hold values from 0.1 to 1.9
- expert_ids: int32 [4096, 2], P('ep'), may hold values from 0 to 31, all different within a row; in each aligned block of 128 rows (0 to 127, 128 to 255, ...) at most 16 rows name the same one
- route_weight: float32 [4096, 2], P('ep'), may hold values from 0.2 to 1
- gate_weight: bfloat16 [32, 2048, 1024], P('ep', None, 'tp'), may hold values from -0.125 to 0.125
- up_weight: bfloat16 [32, 2048, 1024], P('ep', None, 'tp'), may hold values from -0.125 to 0.125
- down_weight: bfloat16 [32, 1024, 2048], P('ep', 'tp'), may hold values from -0.1875 to 0.1875
- shared_gate: bfloat16 [2048, 1024], P(None, 'tp'), may hold values from -0.125 to 0.125
- shared_up: bfloat16 [2048, 1024], P(None, 'tp'), may hold values from -0.125 to 0.125
- shared_down: bfloat16 [1024, 2048], P('tp'), may hold values from -0.1875 to 0.1875
Outputs:
- mixer_out: bfloat16 [4096, 2048], P(('ep', 'tp'))
- expert_out: bfloat16 [4096, 2048], P(('ep', 'tp'))
Inputs may be any that keep to these rules, and one draw needn't show every extreme that they name: `expert_ids`: each row names 2 different experts. In each aligned block of 128 rows no expert is named by more than 16 rows, a bound that some block reaches.
All inputs are finite; a program needn't handle non-finite values.
Results may differ from a plain program's by a relative error of at most 0.012.
The roundings to bfloat16 on the way count: a program that leaves them out, or rounds other values in their place, can miss the bound.
Values may be sent and summed in bfloat16 or wider, within the bound.
A program may use at most 128 MiB of HBM per device.

v0:
```python
import jax
import jax.numpy as jnp
from jax import lax
from jax.sharding import PartitionSpec as P

HEADS = 32
KV_HEADS = 8
HEAD_DIM = 64
WINDOW = 128
BLOCK = 128
TOP_K = 2


epsilon = 1e-06
masked_score = -1e30
score_scale = 0.125


def from_behind(block, axis, distance):
    devices = range(lax.axis_size(axis))
    route = [(i - distance, i) for i in devices if i - distance in devices]
    return lax.ppermute(block, axis, route)


def rms_scale(values, gain):
    widened = values.astype(jnp.float32)
    scaled = widened * lax.rsqrt(jnp.mean(widened * widened, axis=-1, keepdims=True) + epsilon)
    return (scaled * gain).astype(jnp.bfloat16)


def window_mask(first_block, block_count):
    query_pos = jnp.arange(BLOCK)[:, None]
    key_pos = jnp.arange(2 * BLOCK)[None, :]
    inside = (key_pos <= query_pos + BLOCK) & (key_pos > query_pos + BLOCK - WINDOW)
    not_first = (first_block + jnp.arange(block_count))[:, None, None] > 0
    return inside[None] & (not_first | (key_pos[None] >= BLOCK))


def band_blocks(rim_block, blocks_in):
    joined = jnp.concatenate([rim_block[None], blocks_in], axis=0)
    return jnp.concatenate([joined[:-1], joined[1:]], axis=1)


def shards(
    query_rows,
    key_rows,
    value_rows,
    query_gain,
    key_gain,
    sink_logit,
    out_weight,
    tokens,
    norm_gain,
    expert_ids,
    route_weight,
    gate_weight,
    up_weight,
    down_weight,
    shared_gate,
    shared_up,
    shared_down,
):
    expert_ranks = lax.axis_size("ep")
    head_ranks = lax.axis_size("tp")
    head_rank = lax.axis_index("tp")
    sequence_rows = query_rows.shape[0]
    blocks = sequence_rows // BLOCK
    pair_heads = key_rows.shape[1] // HEAD_DIM
    group_size = HEADS // KV_HEADS
    query_normed = rms_scale(
        query_rows.reshape(blocks, BLOCK, pair_heads, group_size, HEAD_DIM), query_gain
    )
    key_normed = rms_scale(key_rows.reshape(blocks, BLOCK, pair_heads, HEAD_DIM), key_gain)
    value_blocks = value_rows.reshape(blocks, BLOCK, pair_heads, HEAD_DIM)
    rim_keys, rim_values = from_behind((key_normed[blocks - 1], value_blocks[blocks - 1]), "ep", 1)
    key_band = band_blocks(rim_keys, key_normed)
    value_band = band_blocks(rim_values, value_blocks)
    window = window_mask(lax.axis_index("ep") * blocks, blocks)
    scores = (
        jnp.einsum("nqhgd,nkhd->hgnqk", query_normed, key_band, preferred_element_type=jnp.float32)
        * score_scale
    )
    scores = jnp.where(window[None, None], scores, masked_score)
    sink_col = sink_logit.reshape(pair_heads, group_size, 1, 1, 1)
    row_max = jnp.maximum(jnp.max(scores, axis=-1, keepdims=True), sink_col)
    exp_scores = jnp.exp(scores - row_max)
    attn_probs = (
        exp_scores / (jnp.sum(exp_scores, axis=-1, keepdims=True) + jnp.exp(sink_col - row_max))
    ).astype(jnp.bfloat16)
    heads_out = (
        jnp.einsum("hgnqk,nkhd->nqhgd", attn_probs, value_band, preferred_element_type=jnp.float32)
        .astype(jnp.bfloat16)
        .reshape(sequence_rows, pair_heads * group_size * HEAD_DIM)
    )
    local_experts = gate_weight.shape[0]
    expert_total = local_experts * expert_ranks
    quarter = tokens.shape[0] // head_ranks
    model_width = tokens.shape[1]
    capacity = 2 * quarter * TOP_K // expert_total
    slot_share = local_experts * capacity
    routed_rows = expert_ranks * slot_share
    normed = rms_scale(tokens, norm_gain)
    route_ids = expert_ids.reshape(head_ranks, quarter * TOP_K)
    one_hot = (route_ids[:, :, None] == jnp.arange(expert_total, dtype=jnp.int32)).astype(jnp.int32)
    slot_rank = jnp.sum(one_hot * (jnp.cumsum(one_hot, axis=1) - 1), axis=-1)
    positions = route_ids * capacity + slot_rank
    owners = jnp.arange(quarter * TOP_K, dtype=jnp.int32) // TOP_K
    padded_rows = jnp.concatenate(
        [
            normed.reshape(head_ranks, quarter, model_width),
            jnp.zeros((head_ranks, 1, model_width), jnp.bfloat16),
        ],
        axis=1,
    ).reshape(head_ranks * (quarter + 1), model_width)
    slot_token = (
        jnp.full((head_ranks, routed_rows), quarter, jnp.int32)
        .at[jnp.arange(head_ranks, dtype=jnp.int32)[:, None], positions]
        .set(jnp.broadcast_to(owners[None, :], positions.shape))
    )
    slot_index = slot_token + (jnp.arange(head_ranks, dtype=jnp.int32) * (quarter + 1))[:, None]
    own_index = lax.dynamic_index_in_dim(slot_index, head_rank, 0, keepdims=True)
    outgoing = padded_rows[own_index].reshape(1, expert_ranks, slot_share, model_width)
    arrived = lax.all_to_all(outgoing, "ep", split_axis=1, concat_axis=1, tiled=True)
    piece_rows = lax.all_gather(
        arrived.reshape(1, expert_ranks, local_experts, capacity, model_width),
        "tp",
        axis=0,
        tiled=True,
    )
    gate_part = jnp.einsum(
        "tsecd,edf->tsecf", piece_rows, gate_weight, preferred_element_type=jnp.float32
    )
    up_part = jnp.einsum(
        "tsecd,edf->tsecf", piece_rows, up_weight, preferred_element_type=jnp.float32
    )
    hidden = (jax.nn.silu(gate_part) * up_part).astype(jnp.bfloat16)
    shared_hidden = (
        jax.nn.silu(jnp.dot(normed, shared_gate, preferred_element_type=jnp.float32))
        * jnp.dot(normed, shared_up, preferred_element_type=jnp.float32)
    ).astype(jnp.bfloat16)
    span_rows = routed_rows + quarter
    mixer_out = lax.psum_scatter(
        jnp.dot(heads_out, out_weight, preferred_element_type=jnp.float32).astype(jnp.bfloat16),
        "tp",
        scatter_dimension=0,
        tiled=True,
    )
    part_count = lax.axis_size("tp") * span_rows // span_rows
    routed_part = jnp.einsum(
        "tsecf,efd->tsecd", hidden, down_weight, preferred_element_type=jnp.float32
    ).reshape(part_count, routed_rows, model_width)
    shared_part = jnp.dot(shared_hidden, shared_down, preferred_element_type=jnp.float32).reshape(
        part_count, quarter, model_width
    )
    summed = lax.psum_scatter(
        jnp.concatenate([routed_part, shared_part], axis=1)
        .reshape(part_count * span_rows, model_width)
        .astype(jnp.bfloat16),
        "tp",
        scatter_dimension=0,
        tiled=True,
    )
    returned = lax.all_to_all(
        summed[:routed_rows].reshape(expert_ranks, slot_share, model_width),
        "ep",
        split_axis=0,
        concat_axis=0,
        tiled=True,
    ).reshape(routed_rows, model_width)
    own_positions = lax.dynamic_index_in_dim(positions, head_rank, 0, keepdims=False)
    picked = returned[own_positions].reshape(quarter, TOP_K, model_width).astype(jnp.float32)
    own_weights = lax.dynamic_slice_in_dim(route_weight, head_rank * quarter, quarter, 0)
    expert_out = (
        summed[routed_rows:].astype(jnp.float32) + jnp.sum(picked * own_weights[:, :, None], axis=1)
    ).astype(jnp.bfloat16)
    return (mixer_out, expert_out)


def solution(mesh):
    in_specs = (
        P("ep", "tp"),
        P("ep", "tp"),
        P("ep", "tp"),
        P(),
        P(),
        P("tp"),
        P("tp", None),
        P("ep", None),
        P(),
        P("ep", None),
        P("ep", None),
        P("ep", None, "tp"),
        P("ep", None, "tp"),
        P("ep", "tp", None),
        P(None, "tp"),
        P(None, "tp"),
        P("tp", None),
    )
    out_specs = (P(("ep", "tp"), None), P(("ep", "tp"), None))
    return jax.shard_map(shards, mesh=mesh, in_specs=in_specs, out_specs=out_specs, check_vma=False)
```

profile of v0, /device:TPU:0, one launch (start us, length us, event | category | flops | bytes accessed | tf_op | source)
XLA Modules:
  0.0 354.6 jit_solution(9129638482711985190)
XLA Ops:
  9.3 2.3 reduce-window.6
  13.8 4.3 %scatter_custom_fusion = s32[2048]{0:T(1024)S(1)} fusion(s32[1024]{0:T(1024)S(1)} %bitcast.147, s32[1024]{0:T(1024)S(1)} %bitcast.148, s32[]{:T(128)} %constant.29.clone.1), kind=kCustom, calls=%fused_computation.89 | custom fusion | bytes 8196
  19.4 2.1 fusion
  21.5 2.1 fusion.2
  23.7 1.4 copy-done.1
  25.1 1.6 concatenate.26
  26.7 3.5 reshape.278
  30.2 7.2 %gather_fusion = bf16[512,2048]{1,0:T(8,128)(2,1)} fusion(bf16[516,2048]{1,0:T(8,128)(2,1)} %reshape.278, s32[1024]{0:T(1024)S(1)} %pad_clamp_fusion.1), kind=kCustom, calls=%fused_computation | custom fusion | bytes 4196352 | tf_op jit(solution)/shard_map/gather | solution.py:122
  37.3 55.5 %all_to_all.10 = bf16[1,8,64,2048]{3,2,0,1:T(8,128)(2,1)S(1)} all-to-all(bf16[1,8,64,2048]{3,2,0,1:T(8,128)(2,1)} %bitcast.138), channel_id=1, replica_groups=mesh['ep'=8,'tp'=4] {'ep'}, dimensions={1} | all-to-all | bytes 4194304 | tf_op jit(solution)/shard_map/all_to_all | solution.py:123
  92.9 1.4 copy.62
  94.6 3.1 fusion.62
  97.7 6.4 %convolution_convert_fusion = bf16[512,2048]{1,0:T(8,128)(2,1)} fusion(bf16[256,2048]{1,0:T(8,128)(2,1)} %param.33, bf16[512,2048]{1,0:T(8,128)(2,1)} %copy-done.1, bf16[2048,256]{1,0:T(8,128)(2,1)} %param.32, f32[512,256]{1,0:T(8,128)} %fusion.62), kind=kOutput, calls=%fused_computation.20 | convolution fusion | flops 1075576832 | bytes 6815744 | tf_op jit(solution)/shard_map/dot_general | solution.py:152
  104.1 47.7 %all-gather.2.cloned.1.call-done = bf16[4,8,4,16,2048]{4,3,1,0,2:T(8,128)(2,1)} async-done(((bf16[1,8,4,16,2048]{4,3,1,0,2:T(8,128)(2,1)}), bf16[4,8,4,16,2048]{4,3,1,0,2:T(8,128)(2,1)}) %all-gather.2.cloned.1.call-update) | async-done | bytes 8388624 | tf_op jit(solution)/shard_map/all_gather | solution.py:124
  151.8 8.3 %fusion.6 = f32[4,4,8,16,256]{4,3,2,1,0:T(8,128)} fusion(bf16[4,8,4,16,2048]{4,3,1,0,2:T(8,128)(2,1)} %all-gather.2.cloned.1.call-done, bf16[4,2048,256]{2,1,0:T(8,128)(2,1)} %param.28), kind=kOutput, calls=%fused_computation.13 | convolution fusion | flops 2147483648 | bytes 14680064 | tf_op jit(solution)/shard_map/tsecd,edf->tsecf/dot_general | solution.py:130
  160.0 14.3 %convert_bitcast_fusion = bf16[4,8,4,16,2048]{4,3,1,0,2:T(8,128)(2,1)} fusion(bf16[4,256,2048]{2,1,0:T(8,128)(2,1)} %param.30, f32[4,4,8,16,256]{4,3,2,1,0:T(8,128)} %fusion.6, bf16[4,8,4,16,2048]{4,3,1,0,2:T(8,128)(2,1)} %all-gather.2.cloned.1.call-done, bf16[4,2048,256]{2,1,0:T(8,128)(2,1)} %param.29), kind=kOutput, calls=%fused_computation.4 | convolution fusion | flops 4302307328 | bytes 27262976 | tf_op jit(solution)/shard_map/tsecf,efd->tsecd/dot_general | solution.py:149
  174.4 8.4 %copy.63 = bf16[4,8,4,16,2048]{4,3,2,1,0:T(8,128)(2,1)} copy(bf16[4,8,4,16,2048]{4,3,1,0,2:T(8,128)(2,1)} %convert_bitcast_fusion) | data formatting | bytes 16777216 | tf_op jit(solution)/shard_map/tsecf,efd->tsecd/transpose | solution.py:149
  182.8 10.5 %pad_maximum_fusion = bf16[4,640,2048]{2,1,0:T(8,128)(2,1)} fusion(bf16[4,128,2048]{2,1,0:T(8,128)(2,1)S(1)} %bitcast.142, bf16[4,512,2048]{2,1,0:T(8,128)(2,1)} %bitcast.137), kind=kLoop, calls=%fused_computation.3 | loop fusion | flops 20971520 | bytes 20971520 | tf_op jit(solution)/shard_map/concatenate | solution.py:156
  194.6 4.0 %collective-permute-start.1 = (bf16[128,2,64]{0,2,1:T(8,128)(2,1)S(1)}, bf16[128,2,64]{0,2,1:T(8,128)(2,1)}, u32[]{:S(2)}, u32[]{:S(2)}) collective-permute-start(bf16[128,2,64]{0,2,1:T(8,128)(2,1)S(1)} %slice_bitcast_fusion), channel_id=1, source_target_pairs={{0,4},{4,8},{8,12},{12,16},{16,20},{20,24},{24,28},{1,5},{5,9},{9,... | collective-permute-start | bytes 98312 | tf_op jit(solution)/shard_map/ppermute | solution.py:22
  198.7 3.0 collective-permute-start
  201.8 1.2 copy.51
  203.0 1.8 reshape.291
  206.9 2.1 fusion.9
  210.1 1.2 fusion.21
  211.7 66.2 %reduce-scatter.5.cloned.1.call-done = bf16[640,2048]{1,0:T(8,128)(2,1)} async-done(((bf16[2560,2048]{1,0:T(8,128)(2,1)}), bf16[640,2048]{1,0:T(8,128)(2,1)}) %reduce-scatter.5.cloned.1.call-update) | async-done | bytes 2621456 | tf_op jit(solution)/shard_map/reduce_scatter | solution.py:155
  277.9 3.2 slice.41
  281.1 5.5 %all-to-all-start.1 = ((bf16[8,64,2048]{2,1,0:T(8,128)(2,1)}), bf16[8,64,2048]{2,1,0:T(8,128)(2,1)}, u32[]{:S(2)}, u32[]{:S(2)}) async-start(bf16[8,64,2048]{2,1,0:T(8,128)(2,1)} %bitcast.139), calls=%async_computation.3 | async-start | bytes 4194304 | tf_op jit(solution)/shard_map/all_to_all | solution.py:163
  286.6 2.6 convolution_convert_fusion.1
  290.1 44.7 %all-to-all-done.1 = bf16[8,64,2048]{2,1,0:T(8,128)(2,1)} async-done(((bf16[8,64,2048]{2,1,0:T(8,128)(2,1)}), bf16[8,64,2048]{2,1,0:T(8,128)(2,1)}, u32[]{:S(2)}, u32[]{:S(2)}) %all-to-all-start.1) | async-done | bytes 2097184 | tf_op jit(solution)/shard_map/all_to_all | solution.py:163
  334.7 4.2 %gather_fusion.1 = bf16[256,2048]{1,0:T(8,128)(2,1)S(1)} fusion(bf16[512,2048]{1,0:T(8,128)(2,1)} %bitcast.31, s32[1024]{0:T(1024)S(1)} %pad_clamp_fusion), kind=kCustom, calls=%fused_computation.1 | custom fusion | bytes 2098176 | tf_op jit(solution)/shard_map/gather | solution.py:171
  339.0 2.3 reshape.292
  341.3 4.8 %multiply_reduce_fusion = f32[128,2048]{1,0:T(8,128)S(1)} fusion(f32[128,2,2048]{2,1,0:T(2,128)} %reshape.292, f32[128,2]{1,0:T(8,128)S(1)} %copy.64), kind=kLoop, calls=%fused_computation.31 | loop fusion | flops 786432 | bytes 3146752 | tf_op jit(solution)/shard_map/reduce_sum | solution.py:174
  346.1 2.0 add_convert_fusion
  (87 shorter events, 11.6 us)
Async XLA Ops:
  7.2 279.4 %copy-start = (bf16[512,2048]{1,0:T(8,128)(2,1)S(1)}, bf16[512,2048]{1,0:T(8,128)(2,1)}, u32[]{:S(2)}) copy-start(bf16[512,2048]{1,0:T(8,128)(2,1)} %param.23) | copy-start | bytes 6291460
  7.2 14.3 %copy-start.6 = (f32[2048]{0:T(1024)S(1)}, f32[2048]{0:T(1024)}, u32[]{:S(2)}) copy-start(f32[2048]{0:T(1024)} %param.25) | copy-start | bytes 24580
  7.2 144.6 %all-gather.2.cloned.1.call-start = ((), (), s32[]{:S(2)}) async-start(), calls=%async_computation.5 | async-start | bytes 10485760 | tf_op jit(solution)/shard_map/all_gather | solution.py:124
  23.7 1.4 copy-start.1
  92.9 1.7 copy-start.9
  94.3 183.5 %reduce-scatter.5.cloned.1.call-start = ((), (), s32[]{:S(2)}) async-start(), calls=%async_computation.6 | async-start | bytes 13107200 | tf_op jit(solution)/shard_map/reduce_scatter | solution.py:155
  174.4 8.4 %copy-start.2 = (bf16[512,2048]{1,0:T(8,128)(2,1)S(1)}, bf16[512,2048]{1,0:T(8,128)(2,1)}, u32[]{:S(2)}) copy-start(bf16[512,2048]{1,0:T(8,128)(2,1)} %convolution_convert_fusion) | copy-start | bytes 6291460
  193.3 0.9 copy-start.5
  193.3 1.2 copy-start.7
  193.3 5.3 %slice-start = ((bf16[512,128]{1,0:T(8,128)(2,1)}), bf16[128,128]{1,0:T(8,128)(2,1)S(1)}, s32[]{:S(2)}) async-start(bf16[512,128]{1,0:T(8,128)(2,1)} %param.19), calls=%async_computation.7 | async-start | bytes 65536 | tf_op jit(solution)/shard_map/slice | solution.py:75
  193.3 8.5 %copy-start.3 = (bf16[512,512]{1,0:T(8,128)(2,1)S(1)}, bf16[512,512]{1,0:T(8,128)(2,1)}, u32[]{:S(2)}) copy-start(bf16[512,512]{1,0:T(8,128)(2,1)} %param.17) | copy-start | bytes 1572868
  194.2 11.0 %copy-start.8 = (f32[64]{0:T(128)S(1)}, f32[64]{0:T(128)}, u32[]{:S(2)}) copy-start(f32[64]{0:T(128)} %param.20) | copy-start | bytes 772
  194.2 12.3 %copy-start.4 = (bf16[512,128]{1,0:T(8,128)(2,1)S(1)}, bf16[512,128]{1,0:T(8,128)(2,1)}, u32[]{:S(2)}) copy-start(bf16[512,128]{1,0:T(8,128)(2,1)} %param.19) | copy-start | bytes 393220
  194.3 12.3 %copy-start.10 = (f32[8]{0:T(128)S(1)}, f32[8]{0:T(128)}, u32[]{:S(2)}) copy-start(f32[8]{0:T(128)} %param.22) | copy-start | bytes 100
  194.6 12.3 %collective-permute-start.1 = (bf16[128,2,64]{0,2,1:T(8,128)(2,1)S(1)}, bf16[128,2,64]{0,2,1:T(8,128)(2,1)}, u32[]{:S(2)}, u32[]{:S(2)}) collective-permute-start(bf16[128,2,64]{0,2,1:T(8,128)(2,1)S(1)} %slice_bitcast_fusion), channel_id=1, source_target_pairs={{0,4},{4,8},{8,12},{12,16},{16,20},{20,24},{24,28},{1,5},{5,9},{9,... | collective-permute-start | bytes 98312 | tf_op jit(solution)/shard_map/ppermute | solution.py:22
  198.7 11.4 %collective-permute-start = (bf16[128,2,64]{0,2,1:T(8,128)(2,1)S(1)}, bf16[128,2,64]{0,2,1:T(8,128)(2,1)S(1)}, u32[]{:S(2)}, u32[]{:S(2)}) collective-permute-start(bf16[128,2,64]{0,2,1:T(8,128)(2,1)S(1)} %bitcast.144), channel_id=1, source_target_pairs={{0,4},{4,8},{8,12},{12,16},{16,20},{20,24},{24,28},{1,5},{5,9},{9,... | collective-permute-start | bytes 98312 | tf_op jit(solution)/shard_map/ppermute | solution.py:22
  281.1 53.7 %all-to-all-start.1 = ((bf16[8,64,2048]{2,1,0:T(8,128)(2,1)}), bf16[8,64,2048]{2,1,0:T(8,128)(2,1)}, u32[]{:S(2)}, u32[]{:S(2)}) async-start(bf16[8,64,2048]{2,1,0:T(8,128)(2,1)} %bitcast.139), calls=%async_computation.3 | async-start | bytes 4194304 | tf_op jit(solution)/shard_map/all_to_all | solution.py:163
  286.5 61.5 %reduce-scatter.3.cloned.1.call-start = ((), (), s32[]{:S(2)}) async-start(), calls=%async_computation.4 | async-start | bytes 2621440 | tf_op jit(solution)/shard_map/reduce_scatter | solution.py:142
Sparse Core Ops, SparseCore 0:
  94.5 57.2 all-gather.1
  193.4 84.4 reduce-scatter.4
  290.4 31.6 reduce-scatter.2
where the time goes:
time: 355 us
  waiting for transfers between devices  159 us (45%)
  blocking collectives  55.5 us (16%)
  local copies, waits for them, and re-layouts  45.8 us (13%)
  matrix products  38 us (11%)
  other arithmetic  29.8 us (8%)
  between operations  14.1 us (4%)
  starting transfers between devices  12.8 us (4%)
    reduce_scatter x1, waiting for transfers between devices, shards(): lax.psum_scatter(jnp.concatenate([routed_part, shared_part], axis=1).resh...  66.2 us
    all_to_all x1, blocking collectives, shards(): lax.all_to_all(outgoing, 'ep', split_axis=1, concat_axis=1, tiled=True)  55.5 us
    all_gather x1, waiting for transfers between devices, shards(): lax.all_gather(arrived.reshape(1, expert_ranks, local_experts, capacity,...  47.7 us
    all_to_all x1, waiting for transfers between devices, shards(): lax.all_to_all(summed[:routed_rows].reshape(expert_ranks, slot_share, mod...  44.7 us
    dot_general x1, matrix products, shards(): jnp.einsum('tsecf,efd->tsecd', hidden, down_weight, preferred_element_typ...  14.3 us
    concatenate x1, other arithmetic, shards(): jnp.concatenate([routed_part, shared_part], axis=1)  10.5 us
    transpose x1, local copies, waits for them, and re-layouts, shards(): jnp.einsum('tsecf,efd->tsecd', hidden, down_weight, preferred_element_typ...  8.41 us
    dot_general x1, matrix products, shards(): jnp.einsum('tsecd,edf->tsecf', piece_rows, gate_weight, preferred_element...  8.25 us
  transfers between devices with their start and end apart: 6, of which 3 were waited for; matrix products, arithmetic and copies ran while one was open for 10% of the time, Pallas kernels for 0%

commit v1 on v0

--- a/solution.py
+++ b/solution.py
@@ -1,6 +1,9 @@
+import functools
 import jax
 import jax.numpy as jnp
 from jax import lax
+from jax.experimental import pallas as pl
+from jax.experimental.pallas import tpu as pltpu
 from jax.sharding import PartitionSpec as P
 
 HEADS = 32
@@ -41,7 +44,319 @@
     return jnp.concatenate([joined[:-1], joined[1:]], axis=1)
 
 
-def shards(
+def attention_part(query_rows, key_rows, value_rows, query_gain, key_gain, sink_logit):
+    sequence_rows = query_rows.shape[0]
+    blocks = sequence_rows // BLOCK
+    pair_heads = key_rows.shape[1] // HEAD_DIM
+    group_size = HEADS // KV_HEADS
+    query_normed = rms_scale(
+        query_rows.reshape(blocks, BLOCK, pair_heads, group_size, HEAD_DIM), query_gain
+    )
+    key_normed = rms_scale(key_rows.reshape(blocks, BLOCK, pair_heads, HEAD_DIM), key_gain)
+    value_blocks = value_rows.reshape(blocks, BLOCK, pair_heads, HEAD_DIM)
+    rim_keys, rim_values = from_behind((key_normed[blocks - 1], value_blocks[blocks - 1]), "ep", 1)
+    key_band = band_blocks(rim_keys, key_normed)
+    value_band = band_blocks(rim_values, value_blocks)
+    window = window_mask(lax.axis_index("ep") * blocks, blocks)
+    scores = (
+        jnp.einsum("nqhgd,nkhd->hgnqk", query_normed, key_band, preferred_element_type=jnp.float32)
+        * score_scale
+    )
+    scores = jnp.where(window[None, None], scores, masked_score)
+    sink_col = sink_logit.reshape(pair_heads, group_size, 1, 1, 1)
+    row_max = jnp.maximum(jnp.max(scores, axis=-1, keepdims=True), sink_col)
+    exp_scores = jnp.exp(scores - row_max)
+    attn_probs = (
+        exp_scores / (jnp.sum(exp_scores, axis=-1, keepdims=True) + jnp.exp(sink_col - row_max))
+    ).astype(jnp.bfloat16)
+    heads_out = (
+        jnp.einsum("hgnqk,nkhd->nqhgd", attn_probs, value_band, preferred_element_type=jnp.float32)
+        .astype(jnp.bfloat16)
+        .reshape(sequence_rows, pair_heads * group_size * HEAD_DIM)
+    )
+    return heads_out
+
+
+def exchange_kernel(
+    ranks,
+    group,
+    local_experts,
+    capacity,
+    outgoing,
+    mixer_part,
+    shared_part,
+    gate,
+    up,
+    down,
+    returned,
+    mixer_sum,
+    shared_sum,
+    rows,
+    kept,
+    sibling_send,
+    sibling_recv,
+    peer_send,
+    peer_recv,
+    finished,
+    early_recv,
+    early_send,
+    early_peer,
+    out_sems,
+    in_sems,
+    fan_send,
+    fan_recv,
+    add_send,
+    add_recv,
+    back_send,
+    back_recv,
+    early_s,
+    early_r,
+    own_sem,
+):
+    rank = lax.axis_index("ep")
+    part = lax.axis_index("tp")
+    sibling = part + 1 - 2 * lax.rem(part, 2)
+    peer = lax.rem(part + 2, 4)
+    across = 3 - part
+    f32, bf16 = jnp.float32, jnp.bfloat16
+    mesh_ids = pl.DeviceIdType.MESH
+
+    def send(source, target, send_sem, recv_sem, ep_to, tp_to):
+        copy = pltpu.make_async_remote_copy(
+            src_ref=source,
+            dst_ref=target,
+            send_sem=send_sem,
+            recv_sem=recv_sem,
+            device_id=(ep_to, tp_to),
+            device_id_type=mesh_ids,
+        )
+        copy.start()
+        return copy
+
+    barrier = pltpu.get_barrier_semaphore()
+    for k in range(1, ranks):
+        pl.semaphore_signal(
+            barrier, inc=1, device_id=(lax.rem(rank + k, ranks), part), device_id_type=mesh_ids
+        )
+    for other in (sibling, peer):
+        pl.semaphore_signal(barrier, inc=1, device_id=(rank, other), device_id_type=mesh_ids)
+    pl.semaphore_wait(barrier, ranks + 1)
+
+    own = pltpu.make_async_copy(outgoing.at[0], rows.at[0, 0], own_sem)
+    own.start()
+    dispatched = [None] + [
+        send(
+            outgoing.at[k],
+            rows.at[k, 0],
+            out_sems.at[k],
+            in_sems.at[k],
+            lax.rem(rank + k, ranks),
+            part,
+        )
+        for k in range(1, ranks)
+    ]
+    early = []
+    for i, full in enumerate((mixer_part, shared_part)):
+        for j, which in enumerate((across, sibling)):
+            s = 2 * i + j
+            early.append(
+                send(
+                    full.at[which],
+                    early_recv.at[s],
+                    early_s.at[s],
+                    early_r.at[s],
+                    rank,
+                    sibling,
+                )
+            )
+    to_sibling = {}
+    to_peer = {}
+    relayed = {}
+    added = {}
+    peered = {}
+    backs = {}
+
+    def fan_out(k):
+        if k == 0:
+            own.wait()
+        else:
+            dispatched[k].wait_recv()
+        to_peer[k] = send(
+            rows.at[k, 0], rows.at[k, 2], fan_send.at[0, k], fan_recv.at[0, k], rank, peer
+        )
+        to_sibling[k] = send(
+            rows.at[k, 0], rows.at[k, 1], fan_send.at[1, k], fan_recv.at[1, k], rank, sibling
+        )
+
+    def relay(k):
+        to_peer[k].wait_recv()
+        relayed[k] = send(
+            rows.at[k, 2], rows.at[k, 3], fan_send.at[2, k], fan_recv.at[2, k], rank, sibling
+        )
+
+    def early_add():
+        for i, full in enumerate((mixer_part, shared_part)):
+            early[2 * i].wait_recv()
+            early_send[i] = (
+                full[peer].astype(f32) + early_recv[2 * i].astype(f32)
+            ).astype(bf16)
+            early.append(
+                send(
+                    early_send.at[i],
+                    early_peer.at[i],
+                    early_s.at[4 + i],
+                    early_r.at[4 + i],
+                    rank,
+                    peer,
+                )
+            )
+
+    def early_finish():
+        for i, (full, total) in enumerate(((mixer_part, mixer_sum), (shared_part, shared_sum))):
+            early[2 * i + 1].wait_recv()
+            early[4 + i].wait_recv()
+            total[...] = (
+                full[part].astype(f32)
+                + early_recv[2 * i + 1].astype(f32)
+                + early_peer[i].astype(f32)
+            ).astype(bf16)
+
+    def experts(g):
+        first = g * group
+        for k in range(first, first + group):
+            to_sibling[k].wait_recv()
+            relayed[k].wait_recv()
+        width = rows.shape[-1]
+
+        def one(index, carry):
+            at = pl.ds(pl.multiple_of(index * capacity, capacity), capacity)
+            block = rows[first : first + group, :, at, :].reshape(group * 4 * capacity, width)
+            gate_part = jnp.dot(block, gate[index], preferred_element_type=f32)
+            up_part = jnp.dot(block, up[index], preferred_element_type=f32)
+            hidden = (gate_part / (1.0 + jnp.exp(-gate_part)) * up_part).astype(bf16)
+            made = jnp.dot(hidden, down[index], preferred_element_type=f32)
+            made = made.astype(bf16).reshape(group, 4, capacity, width)
+            spot = pl.ds(first, group)
+            kept[spot, 0, at, :] = made[:, 0]
+            sibling_send[spot, 0, at, :] = made[:, 1]
+            kept[spot, 1, at, :] = made[:, 2]
+            sibling_send[spot, 1, at, :] = made[:, 3]
+            return carry
+
+        lax.fori_loop(0, local_experts, one, 0)
+        for k in range(first, first + group):
+            added[k] = send(
+                sibling_send.at[k],
+                sibling_recv.at[k],
+                add_send.at[0, k],
+                add_recv.at[0, k],
+                rank,
+                sibling,
+            )
+
+    def pair_add(k):
+        added[k].wait_recv()
+        peer_send[k] = (kept[k, 1].astype(f32) + sibling_recv[k, 1].astype(f32)).astype(bf16)
+        peered[k] = send(
+            peer_send.at[k], peer_recv.at[k], add_send.at[1, k], add_recv.at[1, k], rank, peer
+        )
+
+    def finish(k):
+        peered[k].wait_recv()
+        total = (
+            kept[k, 0].astype(f32) + sibling_recv[k, 0].astype(f32) + peer_recv[k].astype(f32)
+        ).astype(bf16)
+        if k == 0:
+            returned[0] = total
+        else:
+            finished[k] = total
+            backs[k] = send(
+                finished.at[k],
+                returned.at[k],
+                back_send.at[k],
+                back_recv.at[k],
+                lax.rem(rank + ranks - k, ranks),
+                part,
+            )
+
+    groups = ranks // group
+    for step in range(groups + 4):
+        for stage, work in ((0, fan_out), (1, relay)):
+            g = step - stage
+            if 0 <= g < groups:
+                for k in range(g * group, (g + 1) * group):
+                    work(k)
+        if step == 0:
+            early_add()
+        if 0 <= step - 3 < groups:
+            for k in range((step - 3) * group, (step - 2) * group):
+                pair_add(k)
+        if 0 <= step - 2 < groups:
+            experts(step - 2)
+        if 0 <= step - 4 < groups:
+            for k in range((step - 4) * group, (step - 3) * group):
+                finish(k)
+        if step == 2:
+            early_finish()
+    for k in range(1, ranks):
+        backs[k].wait_recv()
+    for k in range(1, ranks):
+        dispatched[k].wait_send()
+        backs[k].wait_send()
+    for table in (to_peer, to_sibling, relayed, added, peered):
+        for k in range(ranks):
+            table[k].wait_send()
+    for copy in early:
+        copy.wait_send()
+
+
+def exchange(outgoing, mixer_part, shared_part, gate, up, down, capacity):
+    ranks, share, width = outgoing.shape
+    quarter = mixer_part.shape[1]
+    local_experts = gate.shape[0]
+    group = 2
+    bf16 = jnp.bfloat16
+    dma = pltpu.SemaphoreType.DMA
+    vmem = pl.BlockSpec(memory_space=pltpu.VMEM)
+    return pl.pallas_call(
+        functools.partial(exchange_kernel, ranks, group, local_experts, capacity),
+        out_shape=(
+            jax.ShapeDtypeStruct((ranks, share, width), bf16),
+            jax.ShapeDtypeStruct((quarter, width), bf16),
+            jax.ShapeDtypeStruct((quarter, width), bf16),
+        ),
+        in_specs=[vmem] * 6,
+        out_specs=(vmem,) * 3,
+        scratch_shapes=[
+            pltpu.VMEM((ranks, 4, share, width), bf16),
+            pltpu.VMEM((ranks, 2, share, width), bf16),
+            pltpu.VMEM((ranks, 2, share, width), bf16),
+            pltpu.VMEM((ranks, 2, share, width), bf16),
+            pltpu.VMEM((ranks, share, width), bf16),
+            pltpu.VMEM((ranks, share, width), bf16),
+            pltpu.VMEM((ranks, share, width), bf16),
+            pltpu.VMEM((4, quarter, width), bf16),
+            pltpu.VMEM((2, quarter, width), bf16),
+            pltpu.VMEM((2, quarter, width), bf16),
+            dma((ranks,)),
+            dma((ranks,)),
+            dma((3, ranks)),
+            dma((3, ranks)),
+            dma((2, ranks)),
+            dma((2, ranks)),
+            dma((ranks,)),
+            dma((ranks,)),
+            dma((6,)),
+            dma((6,)),
+            dma,
+        ],
+        compiler_params=pltpu.CompilerParams(
+            collective_id=0, has_side_effects=True, vmem_limit_bytes=64000 * 1024
+        ),
+    )(outgoing, mixer_part, shared_part, gate, up, down)
+
+
+def wide_shards(
     query_rows,
     key_rows,
     value_rows,
@@ -176,6 +491,106 @@
     return (mixer_out, expert_out)
 
 
+def shards(
+    query_rows,
+    key_rows,
+    value_rows,
+    query_gain,
+    key_gain,
+    sink_logit,
+    out_weight,
+    tokens,
+    norm_gain,
+    expert_ids,
+    route_weight,
+    gate_weight,
+    up_weight,
+    down_weight,
+    shared_gate,
+    shared_up,
+    shared_down,
+):
+    expert_ranks = lax.axis_size("ep")
+    head_ranks = lax.axis_size("tp")
+    head_rank = lax.axis_index("tp")
+    local_experts = gate_weight.shape[0]
+    expert_total = local_experts * expert_ranks
+    quarter = tokens.shape[0] // head_ranks
+    model_width = tokens.shape[1]
+    capacity = 2 * quarter * TOP_K // expert_total
+    if head_ranks != 4 or capacity % 16 or expert_ranks % 2:
+        return wide_shards(
+            query_rows,
+            key_rows,
+            value_rows,
+            query_gain,
+            key_gain,
+            sink_logit,
+            out_weight,
+            tokens,
+            norm_gain,
+            expert_ids,
+            route_weight,
+            gate_weight,
+            up_weight,
+            down_weight,
+            shared_gate,
+            shared_up,
+            shared_down,
+        )
+    slot_share = local_experts * capacity
+    routed_rows = expert_ranks * slot_share
+    heads_out = attention_part(query_rows, key_rows, value_rows, query_gain, key_gain, sink_logit)
+    mixer_part = jnp.dot(heads_out, out_weight, preferred_element_type=jnp.float32).astype(
+        jnp.bfloat16
+    )
+    normed = rms_scale(tokens, norm_gain)
+    shared_hidden = (
+        jax.nn.silu(jnp.dot(normed, shared_gate, preferred_element_type=jnp.float32))
+        * jnp.dot(normed, shared_up, preferred_element_type=jnp.float32)
+    ).astype(jnp.bfloat16)
+    shared_part = jnp.dot(shared_hidden, shared_down, preferred_element_type=jnp.float32).astype(
+        jnp.bfloat16
+    )
+    own_ids = lax.dynamic_slice_in_dim(expert_ids, head_rank * quarter, quarter, 0)
+    own_normed = lax.dynamic_slice_in_dim(normed, head_rank * quarter, quarter, 0)
+    own_weights = lax.dynamic_slice_in_dim(route_weight, head_rank * quarter, quarter, 0)
+    earlier = jnp.arange(quarter)[None, :] < jnp.arange(quarter)[:, None]
+    columns = [own_ids[:, i] for i in range(TOP_K)]
+    positions = []
+    for ids in columns:
+        rank_in = sum(
+            jnp.sum(((ids[:, None] == other[None, :]) & earlier).astype(jnp.int32), axis=1)
+            for other in columns
+        )
+        ahead = lax.rem(ids // local_experts - lax.axis_index("ep") + expert_ranks, expert_ranks)
+        positions.append(ahead * slot_share + lax.rem(ids, local_experts) * capacity + rank_in)
+    slots = jnp.arange(routed_rows, dtype=jnp.int32)
+    chosen = sum((slots[:, None] == spot[None, :]).astype(jnp.bfloat16) for spot in positions)
+    outgoing = jnp.dot(chosen, own_normed, preferred_element_type=jnp.float32).astype(jnp.bfloat16)
+    returned, mixer_out, shared_out = exchange(
+        outgoing.reshape(expert_ranks, slot_share, model_width),
+        mixer_part.reshape(head_ranks, quarter, model_width),
+        shared_part.reshape(head_ranks, quarter, model_width),
+        gate_weight,
+        up_weight,
+        down_weight,
+        capacity,
+    )
+    returned = returned.reshape(routed_rows, model_width)
+    routed = sum(
+        jnp.dot(
+            (spot[:, None] == slots[None, :]).astype(jnp.bfloat16),
+            returned,
+            preferred_element_type=jnp.float32,
+        )
+        * own_weights[:, i : i + 1]
+        for i, spot in enumerate(positions)
+    )
+    expert_out = (shared_out.astype(jnp.float32) + routed).astype(jnp.bfloat16)
+    return (mixer_out, expert_out)
+
+
 def solution(mesh):
     in_specs = (
         P("ep", "tp"),

time: 355 us -> 188 us (0.53)
  waiting for transfers between devices: 159 us -> 0.01 us
  Pallas kernels: 0 us -> 145 us
  blocking collectives: 55.5 us -> 0 us
  local copies, waits for them, and re-layouts: 45.8 us -> 6.85 us
  other arithmetic: 29.8 us -> 6.53 us
  matrix products: 38 us -> 19.8 us
  between operations: 14.1 us -> 0.92 us
  starting transfers between devices: 12.8 us -> 8.92 us
    pallas_call x0 -> x1, Pallas kernels: none -> 145 us  [exchange(): pl.pallas_call(functools.partial(exchange_kernel, ranks, group, local_exp...]
    reduce_scatter x2 -> x0, waiting for transfers between devices: 66.2 us -> none  [the longest x1 66.2 us: shards(): lax.psum_scatter(jnp.concatenate([routed_part, shared_part], axis=1).resh...]
    all_to_all x1 -> x0, blocking collectives: 55.5 us -> none  [shards(): lax.all_to_all(outgoing, 'ep', split_axis=1, concat_axis=1, tiled=True)]
    all_gather x1 -> x0, waiting for transfers between devices: 47.7 us -> none  [shards(): lax.all_gather(arrived.reshape(1, expert_ranks, local_experts, capacity,...]
    all_to_all x1 -> x0, waiting for transfers between devices: 44.7 us -> none  [shards(): lax.all_to_all(summed[:routed_rows].reshape(expert_ranks, slot_share, mod...]
    dot_general x4 -> x5, matrix products: 25.9 us -> 10.7 us  [the longest x2 4.63 us: shards(): jnp.dot((spot[:, None] == slots[None, :]).astype(jnp.bfloat16), returned,...]
    gather x2 -> x0, local copies, waits for them, and re-layouts: 11.4 us -> none  [the longest x1 7.16 us: shards(): padded_rows[own_index].reshape(1, expert_ranks, slot_share, model_width)]
    concatenate x1 -> x0, other arithmetic: 10.5 us -> none  [shards(): jnp.concatenate([routed_part, shared_part], axis=1)]
  transfers between devices with their start and end apart: 6 -> 2, of which waited for: 3 -> 0; matrix products, arithmetic and copies ran while one was open for 10% -> 11% of each run, Pallas kernels for 0% -> 0%
where the time goes in v1:
time: 188 us
  Pallas kernels  145 us (77%)
  matrix products  19.8 us (11%)
  starting transfers between devices  8.92 us (5%)
  local copies, waits for them, and re-layouts  6.85 us (4%)
  other arithmetic  6.53 us (3%)
    pallas_call x1, Pallas kernels, exchange(): pl.pallas_call(functools.partial(exchange_kernel, ranks, group, local_exp...  145 us
    ppermute x2, starting transfers between devices, from_behind(): return lax.ppermute(block, axis, route)  8.92 us
    dot_general x1, matrix products, shards(): jnp.dot(shared_hidden, shared_down, preferred_element_type=jnp.float32)  4.99 us
    dot_general x2, matrix products, shards(): jnp.dot((spot[:, None] == slots[None, :]).astype(jnp.bfloat16), returned,...  4.63 us
  transfers between devices with their start and end apart: 2, of which 0 were waited for; matrix products, arithmetic and copies ran while one was open for 11% of the time, Pallas kernels for 0%

profile of v1, /device:TPU:0, one launch (start us, length us, event | category | flops | bytes accessed | tf_op | source)
XLA Modules:
  0.0 187.6 jit_solution(3570577985190534816)
XLA Ops:
  0.7 0.9 slice.27
  1.5 0.7 copy.34
  2.2 5.5 %collective-permute-start = (bf16[128,2,64]{0,2,1:T(8,128)(2,1)}, bf16[128,2,64]{0,2,1:T(8,128)(2,1)}, u32[]{:S(2)}, u32[]{:S(2)}) collective-permute-start(bf16[128,2,64]{0,2,1:T(8,128)(2,1)} %bitcast.3), channel_id=1, source_target_pairs={{0,4},{4,8},{8,12},{12,16},{16,20},{20,24},{24,28},{1,5},{5,9},{9,... | collective-permute-start | bytes 98312 | tf_op jit(solution)/shard_map/ppermute | solution.py:25
  7.7 1.0 copy.38
  8.8 0.1 reshape.287
  9.0 0.7 fusion.38
  9.7 0.6 slice_bitcast_fusion
  10.3 3.4 %collective-permute-start.1 = (bf16[128,2,64]{0,2,1:T(8,128)(2,1)}, bf16[128,2,64]{0,2,1:T(8,128)(2,1)}, u32[]{:S(2)}, u32[]{:S(2)}) collective-permute-start(bf16[128,2,64]{0,2,1:T(8,128)(2,1)} %slice_bitcast_fusion), channel_id=1, source_target_pairs={{0,4},{4,8},{8,12},{12,16},{16,20},{20,24},{24,28},{1,5},{5,9},{9,... | collective-permute-start | bytes 98312 | tf_op jit(solution)/shard_map/ppermute | solution.py:25
  13.7 0.7 constant_dynamic-slice_fusion.1
  14.4 0.2 convert_reduce_fusion.2
  14.7 0.7 constant_dynamic-slice_fusion
  15.4 2.1 %fusion = f32[512]{0:T(512)S(1)} fusion(bf16[512,2048]{1,0:T(8,128)(2,1)} %param.24), kind=kLoop, calls=%fused_computation.2 | loop fusion | flops 3145216 | bytes 2099200 | tf_op jit(solution)/shard_map/reduce_sum | solution.py:30
  17.6 0.2 copy.41
  17.8 0.4 reshape.288
  18.2 0.2 multiply_reduce_fusion
  18.5 0.2 broadcast_and_fusion
  18.7 1.1 multiply_convert_fusion
  19.8 0.5 fusion.2
  20.4 1.5 fusion.76
  21.9 2.1 %convolution_convert_fusion.1 = bf16[512,2048]{1,0:T(8,128)(2,1)} fusion(bf16[512,2048]{1,0:T(8,128)(2,1)S(1)} %fusion.2, s32[]{:T(128)S(6)} %select_n.31, s32[128]{0:T(128)S(1)} %get-tuple-element.17, s32[128]{0:T(128)S(1)} %get-tuple-element.16), kind=kOutput, calls=%fused_computation.11 | convolution fusion | flops 270008320 | bytes 2622468 | tf_op jit(solution)/shard_map/dot_general | solution.py:570
  23.9 5.0 %convolution_convert_fusion = bf16[512,2048]{1,0:T(8,128)(2,1)} fusion(bf16[256,2048]{1,0:T(8,128)(2,1)S(1)} %copy-done, bf16[512,2048]{1,0:T(8,128)(2,1)S(1)} %fusion.2, bf16[2048,256]{1,0:T(8,128)(2,1)} %param.32, f32[512,256]{1,0:T(8,128)} %fusion.76), kind=kOutput, calls=%fused_computation.10 | convolution fusion | flops 1075576832 | bytes 6815744 | tf_op jit(solution)/shard_map/dot_general | solution.py:552
  28.9 0.1 reshape.291
  29.2 0.1 copy.36
  29.3 1.9 %fusion.4 = (f32[2,4,4,128]{3,1,2,0:T(4,128)S(1)}, f32[2,4,256,128,4]{3,2,4,1,0:T(8,128)S(1)}) fusion(pred[4,128,256]{1,2,0:T(8,128)(4,1)S(1)} %broadcast_and_fusion, bf16[4,128,2,4,64]{1,0,4,3,2:T(4,128)(2,1)} %multiply_convert_fusion, bf16[4,128,2,64]{1,3,0,2:T(8,128)(2,1)S(1)} %fusion.38, bf16[1,128,2,64]{1,3,0,2:T(8,128)(2,1)} %bitcast.8), kind=kOutput, calls=%fused_computation.9 | convolution fusion | flops 138145792 | bytes 5029888 | tf_op jit(solution)/shard_map/nqhgd,nkhd->hgnqk/dot_general | solution.py:62
  31.3 1.0 fusion.3
  32.4 2.1 %fusion.13 = bf16[4,128,2,4,64]{1,4,3,2,0:T(8,128)(2,1)S(1)} fusion(bf16[4,128,2,64]{1,3,2,0:T(8,128)(2,1)S(1)} %copy.36, bf16[1,128,2,64]{1,3,2,0:T(8,128)(2,1)} %bitcast.4, f32[2,4,256,128,4]{3,2,4,1,0:T(8,128)S(1)} %get-tuple-element.21, f32[2,4,4,128]{3,1,2,0:T(4,128)S(1)} %exponential_add_fusion, f32[2,4,4,128]{3,1,2,0:T(4,128)S(1)} %broadcast_maximum_fusion, ...), kind=kOutput, calls=%fused_computation.22 | convolution fusion | flops 140509184 | bytes 5046272 | tf_op jit(solution)/shard_map/hgnqk,nkhd->nqhgd/dot_general | solution.py:73
  34.5 0.4 copy.44
  34.9 2.6 %convolution_convert_fusion.2 = bf16[512,2048]{1,0:T(8,128)(2,1)} fusion(bf16[512,2048]{1,0:T(8,128)(2,1)S(1)} %copy-done.8, bf16[64,8,4,128]{3,2,1,0:T(4,128)(2,1)S(1)} %bitcast.83), kind=kOutput, calls=%fused_computation.12 | convolution fusion | flops 1074790400 | bytes 4718592 | tf_op jit(solution)/shard_map/dot_general | solution.py:544
  37.6 144.6 %shard_map.176 = (bf16[8,64,2048]{2,1,0:T(8,128)(2,1)}, bf16[128,2048]{1,0:T(8,128)(2,1)}, bf16[128,2048]{1,0:T(8,128)(2,1)}) custom-call(bf16[8,64,2048]{2,1,0:T(8,128)(2,1)} %bitcast.78, bf16[4,128,2048]{2,1,0:T(8,128)(2,1)} %bitcast.82, bf16[4,128,2048]{2,1,0:T(8,128)(2,1)} %bitcast.81, bf16[4,2048,256]{2,1,0:T(8,128)(2,1)} %gate.1, ...), custom_call_target="tpu_custom_call" | custom-call | tf_op jit(solution)/shard_map/pallas_call | solution.py:321
  182.2 2.2 %convolution_multiply_fusion.1 = f32[128,2048]{1,0:T(8,128)S(1)} fusion(bf16[512,2048]{1,0:T(8,128)(2,1)} %bitcast.79, f32[128]{0:T(128)S(1)} %get-tuple-element.15, s32[128]{0:T(128)S(1)} %get-tuple-element.13), kind=kOutput, calls=%fused_computation.16 | convolution fusion | flops 268763136 | bytes 3146752 | tf_op jit(solution)/shard_map/dot_general | solution.py:582
  184.4 2.4 %fusion.7 = bf16[128,2048]{1,0:T(8,128)(2,1)} fusion(f32[128,2048]{1,0:T(8,128)S(1)} %convolution_multiply_fusion.1, bf16[512,2048]{1,0:T(8,128)(2,1)S(1)} %bitcast.80, bf16[128,2048]{1,0:T(8,128)(2,1)} %get-tuple-element.6, f32[128]{0:T(128)S(1)} %get-tuple-element.14, s32[128]{0:T(128)S(1)} %get-tuple-element.12), kind=kOutput, calls=%fused_computation.17 | convolution fusion | flops 269811712 | bytes 4195328 | tf_op jit(solution)/shard_map/dot_general | solution.py:582
  186.8 0.8 copy.73
  (40 shorter events, 0.6 us)
Async XLA Ops:
  0.6 23.3 %copy-start = (bf16[256,2048]{1,0:T(8,128)(2,1)S(1)}, bf16[256,2048]{1,0:T(8,128)(2,1)}, u32[]{:S(2)}) copy-start(bf16[256,2048]{1,0:T(8,128)(2,1)} %param.33) | copy-start | bytes 3145732
  0.6 16.9 %copy-start.3 = (bf16[512,512]{1,0:T(8,128)(2,1)S(1)}, bf16[512,512]{1,0:T(8,128)(2,1)}, u32[]{:S(2)}) copy-start(bf16[512,512]{1,0:T(8,128)(2,1)} %param.17) | copy-start | bytes 1572868
  2.2 30.1 %collective-permute-start = (bf16[128,2,64]{0,2,1:T(8,128)(2,1)}, bf16[128,2,64]{0,2,1:T(8,128)(2,1)}, u32[]{:S(2)}, u32[]{:S(2)}) collective-permute-start(bf16[128,2,64]{0,2,1:T(8,128)(2,1)} %bitcast.3), channel_id=1, source_target_pairs={{0,4},{4,8},{8,12},{12,16},{16,20},{20,24},{24,28},{1,5},{5,9},{9,... | collective-permute-start | bytes 98312 | tf_op jit(solution)/shard_map/ppermute | solution.py:25
  8.8 9.9 %copy-start.7 = (f32[64]{0:T(128)S(1)}, f32[64]{0:T(128)}, u32[]{:S(2)}) copy-start(f32[64]{0:T(128)} %param.20) | copy-start | bytes 772
  10.3 19.0 %collective-permute-start.1 = (bf16[128,2,64]{0,2,1:T(8,128)(2,1)}, bf16[128,2,64]{0,2,1:T(8,128)(2,1)}, u32[]{:S(2)}, u32[]{:S(2)}) collective-permute-start(bf16[128,2,64]{0,2,1:T(8,128)(2,1)} %slice_bitcast_fusion), channel_id=1, source_target_pairs={{0,4},{4,8},{8,12},{12,16},{16,20},{20,24},{24,28},{1,5},{5,9},{9,... | collective-permute-start | bytes 98312 | tf_op jit(solution)/shard_map/ppermute | solution.py:25
  15.4 4.4 %copy-start.6 = (f32[2048]{0:T(1024)S(1)}, f32[2048]{0:T(1024)}, u32[]{:S(2)}) copy-start(f32[2048]{0:T(1024)} %param.25) | copy-start | bytes 24580
  18.1 1.7 copy-start.2
  18.2 2.2 %copy-start.9 = (bf16[2048,256]{1,0:T(8,128)(2,1)S(1)}, bf16[2048,256]{1,0:T(8,128)(2,1)}, u32[]{:S(2)}) copy-start(bf16[2048,256]{1,0:T(8,128)(2,1)} %param.31) | copy-start | bytes 3145732
  23.9 5.0 %copy-start.5 = (bf16[512,128]{1,0:T(8,128)(2,1)S(1)}, bf16[512,128]{1,0:T(8,128)(2,1)}, u32[]{:S(2)}) copy-start(bf16[512,128]{1,0:T(8,128)(2,1)} %param.19) | copy-start | bytes 393220
  23.9 5.1 %copy-start.10 = (f32[8]{0:T(128)S(1)}, f32[8]{0:T(128)}, u32[]{:S(2)}) copy-start(f32[8]{0:T(128)} %param.22) | copy-start | bytes 100
  32.4 2.5 %copy-start.8 = (bf16[512,2048]{1,0:T(8,128)(2,1)S(1)}, bf16[512,2048]{1,0:T(8,128)(2,1)}, u32[]{:S(2)}) copy-start(bf16[512,2048]{1,0:T(8,128)(2,1)} %param.23) | copy-start | bytes 6291460
  182.2 2.3 %copy-start.1 = (bf16[8,64,2048]{2,1,0:T(8,128)(2,1)S(1)}, bf16[8,64,2048]{2,1,0:T(8,128)(2,1)}, u32[]{:S(2)}) copy-start(bf16[8,64,2048]{2,1,0:T(8,128)(2,1)} %get-tuple-element.7) | copy-start | bytes 6291460
  182.2 4.7 %copy-start.4 = (bf16[128,2048]{1,0:T(8,128)(2,1)S(1)}, bf16[128,2048]{1,0:T(8,128)(2,1)}, u32[]{:S(2)}) copy-start(bf16[128,2048]{1,0:T(8,128)(2,1)} %get-tuple-element.24) | copy-start | bytes 1572868

commit v2 on v1

--- a/solution.py
+++ b/solution.py
@@ -83,11 +83,12 @@
     local_experts,
     capacity,
     outgoing,
+    outgoing_peer,
     mixer_part,
     shared_part,
-    gate,
-    up,
-    down,
+    gate_hbm,
+    up_hbm,
+    down_hbm,
     returned,
     mixer_sum,
     shared_sum,
@@ -112,6 +113,10 @@
     early_s,
     early_r,
     own_sem,
+    gate,
+    up,
+    down,
+    weight_sem,
 ):
     rank = lax.axis_index("ep")
     part = lax.axis_index("tp")
@@ -121,6 +126,12 @@
     f32, bf16 = jnp.float32, jnp.bfloat16
     mesh_ids = pl.DeviceIdType.MESH
 
+    def partner(k, sign=1):
+        half = ranks // 2
+        return lax.rem(rank // 2 + half + sign * (k // 2), half) * 2 + lax.rem(
+            lax.rem(rank, 2) + k, 2
+        )
+
     def send(source, target, send_sem, recv_sem, ep_to, tp_to):
         copy = pltpu.make_async_remote_copy(
             src_ref=source,
@@ -136,7 +147,7 @@
     barrier = pltpu.get_barrier_semaphore()
     for k in range(1, ranks):
         pl.semaphore_signal(
-            barrier, inc=1, device_id=(lax.rem(rank + k, ranks), part), device_id_type=mesh_ids
+            barrier, inc=1, device_id=(partner(k), part), device_id_type=mesh_ids
         )
     for other in (sibling, peer):
         pl.semaphore_signal(barrier, inc=1, device_id=(rank, other), device_id_type=mesh_ids)
@@ -144,13 +155,20 @@
 
     own = pltpu.make_async_copy(outgoing.at[0], rows.at[0, 0], own_sem)
     own.start()
+    to_sibling = {}
+    to_peer = {}
+    to_peer[1] = send(
+        outgoing_peer.at[1], rows.at[1, 2], fan_send.at[0, 1], fan_recv.at[0, 1], partner(1), part
+    )
+    beside = pltpu.make_async_copy(outgoing_peer.at[0], rows.at[0, 2], fan_recv.at[0, 0])
+    beside.start()
     dispatched = [None] + [
         send(
             outgoing.at[k],
             rows.at[k, 0],
             out_sems.at[k],
             in_sems.at[k],
-            lax.rem(rank + k, ranks),
+            partner(k),
             part,
         )
         for k in range(1, ranks)
@@ -169,8 +187,12 @@
                     sibling,
                 )
             )
-    to_sibling = {}
-    to_peer = {}
+    loads = [
+        pltpu.make_async_copy(source, held, weight_sem.at[i])
+        for i, (source, held) in enumerate(((gate_hbm, gate), (up_hbm, up), (down_hbm, down)))
+    ]
+    for load in loads:
+        load.start()
     relayed = {}
     added = {}
     peered = {}
@@ -181,15 +203,19 @@
             own.wait()
         else:
             dispatched[k].wait_recv()
-        to_peer[k] = send(
-            rows.at[k, 0], rows.at[k, 2], fan_send.at[0, k], fan_recv.at[0, k], rank, peer
-        )
+        if k > 1:
+            to_peer[k] = send(
+                rows.at[k, 0], rows.at[k, 2], fan_send.at[0, k], fan_recv.at[0, k], rank, peer
+            )
         to_sibling[k] = send(
             rows.at[k, 0], rows.at[k, 1], fan_send.at[1, k], fan_recv.at[1, k], rank, sibling
         )
 
     def relay(k):
-        to_peer[k].wait_recv()
+        if k == 0:
+            beside.wait()
+        else:
+            to_peer[k].wait_recv()
         relayed[k] = send(
             rows.at[k, 2], rows.at[k, 3], fan_send.at[2, k], fan_recv.at[2, k], rank, sibling
         )
@@ -226,6 +252,9 @@
         for k in range(first, first + group):
             to_sibling[k].wait_recv()
             relayed[k].wait_recv()
+        if g == 0:
+            for load in loads:
+                load.wait()
         width = rows.shape[-1]
 
         def one(index, carry):
@@ -275,7 +304,7 @@
                 returned.at[k],
                 back_send.at[k],
                 back_recv.at[k],
-                lax.rem(rank + ranks - k, ranks),
+                partner(k, -1),
                 part,
             )
 
@@ -304,17 +333,17 @@
         dispatched[k].wait_send()
         backs[k].wait_send()
     for table in (to_peer, to_sibling, relayed, added, peered):
-        for k in range(ranks):
+        for k in table:
             table[k].wait_send()
     for copy in early:
         copy.wait_send()
 
 
-def exchange(outgoing, mixer_part, shared_part, gate, up, down, capacity):
+def exchange(outgoing, outgoing_peer, mixer_part, shared_part, gate, up, down, capacity):
     ranks, share, width = outgoing.shape
     quarter = mixer_part.shape[1]
     local_experts = gate.shape[0]
-    group = 2
+    group = 1
     bf16 = jnp.bfloat16
     dma = pltpu.SemaphoreType.DMA
     vmem = pl.BlockSpec(memory_space=pltpu.VMEM)
@@ -325,7 +354,7 @@
             jax.ShapeDtypeStruct((quarter, width), bf16),
             jax.ShapeDtypeStruct((quarter, width), bf16),
         ),
-        in_specs=[vmem] * 6,
+        in_specs=[vmem] * 4 + [pl.BlockSpec(memory_space=pl.ANY)] * 3,
         out_specs=(vmem,) * 3,
         scratch_shapes=[
             pltpu.VMEM((ranks, 4, share, width), bf16),
@@ -349,11 +378,15 @@
             dma((6,)),
             dma((6,)),
             dma,
+            pltpu.VMEM(gate.shape, bf16),
+            pltpu.VMEM(up.shape, bf16),
+            pltpu.VMEM(down.shape, bf16),
+            dma((3,)),
         ],
         compiler_params=pltpu.CompilerParams(
             collective_id=0, has_side_effects=True, vmem_limit_bytes=64000 * 1024
         ),
-    )(outgoing, mixer_part, shared_part, gate, up, down)
+    )(outgoing, outgoing_peer, mixer_part, shared_part, gate, up, down)
 
 
 def wide_shards(
@@ -552,24 +585,37 @@
     shared_part = jnp.dot(shared_hidden, shared_down, preferred_element_type=jnp.float32).astype(
         jnp.bfloat16
     )
-    own_ids = lax.dynamic_slice_in_dim(expert_ids, head_rank * quarter, quarter, 0)
-    own_normed = lax.dynamic_slice_in_dim(normed, head_rank * quarter, quarter, 0)
+    rank = lax.axis_index("ep")
+    earlier = jnp.arange(quarter)[None, :] < jnp.arange(quarter)[:, None]
+    slots = jnp.arange(routed_rows, dtype=jnp.int32)
+
+    def slot_rows(part, count):
+        own_ids = lax.dynamic_slice_in_dim(expert_ids, part * quarter, quarter, 0)
+        own_normed = lax.dynamic_slice_in_dim(normed, part * quarter, quarter, 0)
+        columns = [own_ids[:, i] for i in range(TOP_K)]
+        positions = []
+        for ids in columns:
+            rank_in = sum(
+                jnp.sum(((ids[:, None] == other[None, :]) & earlier).astype(jnp.int32), axis=1)
+                for other in columns
+            )
+            owner = ids // local_experts
+            half = expert_ranks // 2
+            ahead = 2 * lax.rem(owner // 2 - rank // 2 + half, half) + lax.rem(owner + rank, 2)
+            positions.append(
+                ahead * slot_share + lax.rem(ids, local_experts) * capacity + rank_in
+            )
+        used = slots[: count * slot_share]
+        chosen = sum((used[:, None] == spot[None, :]).astype(jnp.bfloat16) for spot in positions)
+        made = jnp.dot(chosen, own_normed, preferred_element_type=jnp.float32)
+        return positions, made.astype(jnp.bfloat16).reshape(count, slot_share, model_width)
+
+    positions, outgoing = slot_rows(head_rank, expert_ranks)
+    _, outgoing_peer = slot_rows(lax.rem(head_rank + 2, 4), 2)
     own_weights = lax.dynamic_slice_in_dim(route_weight, head_rank * quarter, quarter, 0)
-    earlier = jnp.arange(quarter)[None, :] < jnp.arange(quarter)[:, None]
-    columns = [own_ids[:, i] for i in range(TOP_K)]
-    positions = []
-    for ids in columns:
-        rank_in = sum(
-            jnp.sum(((ids[:, None] == other[None, :]) & earlier).astype(jnp.int32), axis=1)
-            for other in columns
-        )
-        ahead = lax.rem(ids // local_experts - lax.axis_index("ep") + expert_ranks, expert_ranks)
-        positions.append(ahead * slot_share + lax.rem(ids, local_experts) * capacity + rank_in)
-    slots = jnp.arange(routed_rows, dtype=jnp.int32)
-    chosen = sum((slots[:, None] == spot[None, :]).astype(jnp.bfloat16) for spot in positions)
-    outgoing = jnp.dot(chosen, own_normed, preferred_element_type=jnp.float32).astype(jnp.bfloat16)
     returned, mixer_out, shared_out = exchange(
-        outgoing.reshape(expert_ranks, slot_share, model_width),
+        outgoing,
+        outgoing_peer,
         mixer_part.reshape(head_ranks, quarter, model_width),
         shared_part.reshape(head_ranks, quarter, model_width),
         gate_weight,

time: 188 us -> 177 us (0.941)
  Pallas kernels: 145 us -> 131 us
    pallas_call x1, Pallas kernels: 145 us -> 131 us  [exchange(): pl.pallas_call(functools.partial(exchange_kernel, ranks, group, local_exp...]
  transfers between devices with their start and end apart: 2 -> 2, of which waited for: 0 -> 0; matrix products, arithmetic and copies ran while one was open for 11% -> 14% of each run, Pallas kernels for 0% -> 0%
where the time goes in v2:
time: 177 us
  Pallas kernels  131 us (74%)
  matrix products  21 us (12%)
  starting transfers between devices  8.92 us (5%)
  other arithmetic  8.36 us (5%)
  local copies, waits for them, and re-layouts  6.87 us (4%)
    pallas_call x1, Pallas kernels, exchange(): pl.pallas_call(functools.partial(exchange_kernel, ranks, group, local_exp...  131 us
    ppermute x2, starting transfers between devices, from_behind(): return lax.ppermute(block, axis, route)  8.92 us
    dot_general x1, matrix products, shards(): jnp.dot(shared_hidden, shared_down, preferred_element_type=jnp.float32)  4.99 us
    dot_general x2, matrix products, shards(): jnp.dot((spot[:, None] == slots[None, :]).astype(jnp.bfloat16), returned,...  4.63 us
    convert_element_type x3, other arithmetic, rms_scale(): return (scaled * gain).astype(jnp.bfloat16)  3.96 us
  transfers between devices with their start and end apart: 2, of which 0 were waited for; matrix products, arithmetic and copies ran while one was open for 14% of the time, Pallas kernels for 0%

profile of v2, /device:TPU:0, one launch (start us, length us, event | category | flops | bytes accessed | tf_op | source)
XLA Modules:
  0.0 176.6 jit_solution(2282164668483434530)
XLA Ops:
  0.7 0.9 slice.41
  1.5 0.7 copy.34
  2.2 5.5 %collective-permute-start = (bf16[128,2,64]{0,2,1:T(8,128)(2,1)}, bf16[128,2,64]{0,2,1:T(8,128)(2,1)}, u32[]{:S(2)}, u32[]{:S(2)}) collective-permute-start(bf16[128,2,64]{0,2,1:T(8,128)(2,1)} %bitcast.6), channel_id=1, source_target_pairs={{0,4},{4,8},{8,12},{12,16},{16,20},{20,24},{24,28},{1,5},{5,9},{9,... | collective-permute-start | bytes 98312 | tf_op jit(solution)/shard_map/ppermute | solution.py:25
  7.7 1.0 copy.38
  9.0 0.7 fusion.39
  9.7 0.6 slice_bitcast_fusion
  10.3 3.4 %collective-permute-start.1 = (bf16[128,2,64]{0,2,1:T(8,128)(2,1)}, bf16[128,2,64]{0,2,1:T(8,128)(2,1)}, u32[]{:S(2)}, u32[]{:S(2)}) collective-permute-start(bf16[128,2,64]{0,2,1:T(8,128)(2,1)} %slice_bitcast_fusion), channel_id=1, source_target_pairs={{0,4},{4,8},{8,12},{12,16},{16,20},{20,24},{24,28},{1,5},{5,9},{9,... | collective-permute-start | bytes 98312 | tf_op jit(solution)/shard_map/ppermute | solution.py:25
  13.8 2.1 %fusion = f32[512]{0:T(512)S(1)} fusion(bf16[512,2048]{1,0:T(8,128)(2,1)} %param.24), kind=kLoop, calls=%fused_computation.2 | loop fusion | flops 3145216 | bytes 2099200 | tf_op jit(solution)/shard_map/reduce_sum | solution.py:30
  15.9 0.7 constant_dynamic-slice_fusion
  16.6 0.7 constant_dynamic-slice_fusion.1
  17.3 0.2 copy.41
  17.5 0.4 reshape.481
  17.9 0.2 multiply_reduce_fusion
  18.3 0.2 convert_reduce_fusion.2
  18.5 0.2 convert_reduce_fusion.6
  18.7 0.2 broadcast_and_fusion
  18.9 1.1 multiply_convert_fusion
  20.0 2.1 %fusion.2 = bf16[512,2048]{1,0:T(8,128)(2,1)S(1)} fusion(bf16[512,2048]{1,0:T(8,128)(2,1)} %param.24, f32[2048]{0:T(1024)S(1)} %copy-done.5, f32[512]{0:T(512)S(1)} %add_rsqrt_fusion.2), kind=kLoop, calls=%fused_computation.4 | loop fusion | flops 4194304 | bytes 4204544 | tf_op jit(solution)/shard_map/convert_element_type | solution.py:31
  22.2 1.5 fusion.95
  23.8 2.1 %convolution_convert_fusion.1 = bf16[512,2048]{1,0:T(8,128)(2,1)} fusion(bf16[512,2048]{1,0:T(8,128)(2,1)S(1)} %fusion.2, s32[]{:T(128)S(6)} %select_n.91, s32[128]{0:T(128)S(1)} %get-tuple-element.32, s32[128]{0:T(128)S(1)} %get-tuple-element.33), kind=kOutput, calls=%fused_computation.11 | convolution fusion | flops 270008320 | bytes 2622468 | tf_op jit(solution)/shard_map/dot_general | solution.py:610
  25.8 1.1 convolution_convert_fusion.3
  27.0 5.0 %convolution_convert_fusion = bf16[512,2048]{1,0:T(8,128)(2,1)} fusion(bf16[256,2048]{1,0:T(8,128)(2,1)S(1)} %copy-done, bf16[512,2048]{1,0:T(8,128)(2,1)S(1)} %fusion.2, bf16[2048,256]{1,0:T(8,128)(2,1)} %param.32, f32[512,256]{1,0:T(8,128)} %fusion.95), kind=kOutput, calls=%fused_computation.10 | convolution fusion | flops 1075576832 | bytes 6815744 | tf_op jit(solution)/shard_map/dot_general | solution.py:585
  32.2 0.1 copy.36
  32.3 1.9 %fusion.4 = (f32[2,4,4,128]{3,1,2,0:T(4,128)S(1)}, f32[2,4,256,128,4]{3,2,4,1,0:T(8,128)S(1)}) fusion(pred[4,128,256]{1,2,0:T(8,128)(4,1)S(1)} %broadcast_and_fusion, bf16[4,128,2,4,64]{1,0,4,3,2:T(4,128)(2,1)} %multiply_convert_fusion, bf16[4,128,2,64]{1,3,0,2:T(8,128)(2,1)S(1)} %fusion.39, bf16[1,128,2,64]{1,3,0,2:T(8,128)(2,1)} %bitcast.11), kind=kOutput, calls=%fused_computation.9 | convolution fusion | flops 138145792 | bytes 5029888 | tf_op jit(solution)/shard_map/nqhgd,nkhd->hgnqk/dot_general | solution.py:62
  34.3 1.0 fusion.3
  35.4 2.1 %fusion.13 = bf16[4,128,2,4,64]{1,4,3,2,0:T(8,128)(2,1)S(1)} fusion(bf16[4,128,2,64]{1,3,2,0:T(8,128)(2,1)S(1)} %copy.36, bf16[1,128,2,64]{1,3,2,0:T(8,128)(2,1)} %bitcast.7, f32[2,4,256,128,4]{3,2,4,1,0:T(8,128)S(1)} %get-tuple-element.31, f32[2,4,4,128]{3,1,2,0:T(4,128)S(1)} %exponential_add_fusion, f32[2,4,4,128]{3,1,2,0:T(4,128)S(1)} %broadcast_maximum_fusion, ...), kind=kOutput, calls=%fused_computation.23 | convolution fusion | flops 140509184 | bytes 5046272 | tf_op jit(solution)/shard_map/hgnqk,nkhd->nqhgd/dot_general | solution.py:73
  37.5 0.4 copy.44
  38.0 2.6 %convolution_convert_fusion.2 = bf16[512,2048]{1,0:T(8,128)(2,1)} fusion(bf16[512,2048]{1,0:T(8,128)(2,1)S(1)} %copy-done.7, bf16[64,8,4,128]{3,2,1,0:T(4,128)(2,1)S(1)} %bitcast.93), kind=kOutput, calls=%fused_computation.12 | convolution fusion | flops 1074790400 | bytes 4718592 | tf_op jit(solution)/shard_map/dot_general | solution.py:577
  40.6 130.5 %shard_map.176 = (bf16[8,64,2048]{2,1,0:T(8,128)(2,1)}, bf16[128,2048]{1,0:T(8,128)(2,1)}, bf16[128,2048]{1,0:T(8,128)(2,1)}) custom-call(bf16[8,64,2048]{2,1,0:T(8,128)(2,1)} %bitcast.87, bf16[2,64,2048]{2,1,0:T(8,128)(2,1)} %bitcast.92, bf16[4,128,2048]{2,1,0:T(8,128)(2,1)} %bitcast.91, bf16[4,128,2048]{2,1,0:T(8,128)(2,1)} %bitcast.90, ...), custom_call_target="tpu_custom_call" | custom-call | tf_op jit(solution)/shard_map/pallas_call | solution.py:350
  171.1 2.2 %convolution_multiply_fusion.1 = f32[128,2048]{1,0:T(8,128)S(1)} fusion(bf16[512,2048]{1,0:T(8,128)(2,1)} %bitcast.88, f32[128]{0:T(128)S(1)} %get-tuple-element.21, s32[128]{0:T(128)S(1)} %get-tuple-element.19), kind=kOutput, calls=%fused_computation.16 | convolution fusion | flops 268763136 | bytes 3146752 | tf_op jit(solution)/shard_map/dot_general | solution.py:628
  173.4 2.4 %fusion.7 = bf16[128,2048]{1,0:T(8,128)(2,1)} fusion(f32[128,2048]{1,0:T(8,128)S(1)} %convolution_multiply_fusion.1, bf16[512,2048]{1,0:T(8,128)(2,1)S(1)} %bitcast.89, bf16[128,2048]{1,0:T(8,128)(2,1)} %get-tuple-element.6, f32[128]{0:T(128)S(1)} %get-tuple-element.20, s32[128]{0:T(128)S(1)} %get-tuple-element.18), kind=kOutput, calls=%fused_computation.17 | convolution fusion | flops 269811712 | bytes 4195328 | tf_op jit(solution)/shard_map/dot_general | solution.py:628
  175.8 0.8 copy.73
  (43 shorter events, 0.8 us)
Async XLA Ops:
  0.6 26.3 %copy-start = (bf16[256,2048]{1,0:T(8,128)(2,1)S(1)}, bf16[256,2048]{1,0:T(8,128)(2,1)}, u32[]{:S(2)}) copy-start(bf16[256,2048]{1,0:T(8,128)(2,1)} %param.33) | copy-start | bytes 3145732
  0.6 16.7 %copy-start.2 = (bf16[512,512]{1,0:T(8,128)(2,1)S(1)}, bf16[512,512]{1,0:T(8,128)(2,1)}, u32[]{:S(2)}) copy-start(bf16[512,512]{1,0:T(8,128)(2,1)} %param.17) | copy-start | bytes 1572868
  2.2 33.1 %collective-permute-start = (bf16[128,2,64]{0,2,1:T(8,128)(2,1)}, bf16[128,2,64]{0,2,1:T(8,128)(2,1)}, u32[]{:S(2)}, u32[]{:S(2)}) collective-permute-start(bf16[128,2,64]{0,2,1:T(8,128)(2,1)} %bitcast.6), channel_id=1, source_target_pairs={{0,4},{4,8},{8,12},{12,16},{16,20},{20,24},{24,28},{1,5},{5,9},{9,... | collective-permute-start | bytes 98312 | tf_op jit(solution)/shard_map/ppermute | solution.py:25
  8.7 10.2 %copy-start.6 = (f32[64]{0:T(128)S(1)}, f32[64]{0:T(128)}, u32[]{:S(2)}) copy-start(f32[64]{0:T(128)} %param.20) | copy-start | bytes 772
  10.3 22.0 %collective-permute-start.1 = (bf16[128,2,64]{0,2,1:T(8,128)(2,1)}, bf16[128,2,64]{0,2,1:T(8,128)(2,1)}, u32[]{:S(2)}, u32[]{:S(2)}) collective-permute-start(bf16[128,2,64]{0,2,1:T(8,128)(2,1)} %slice_bitcast_fusion), channel_id=1, source_target_pairs={{0,4},{4,8},{8,12},{12,16},{16,20},{20,24},{24,28},{1,5},{5,9},{9,... | collective-permute-start | bytes 98312 | tf_op jit(solution)/shard_map/ppermute | solution.py:25
  13.8 6.2 %copy-start.5 = (f32[2048]{0:T(1024)S(1)}, f32[2048]{0:T(1024)}, u32[]{:S(2)}) copy-start(f32[2048]{0:T(1024)} %param.25) | copy-start | bytes 24580
  18.2 4.0 %copy-start.8 = (bf16[2048,256]{1,0:T(8,128)(2,1)S(1)}, bf16[2048,256]{1,0:T(8,128)(2,1)}, u32[]{:S(2)}) copy-start(bf16[2048,256]{1,0:T(8,128)(2,1)} %param.31) | copy-start | bytes 3145732
  26.9 5.0 %copy-start.4 = (bf16[512,128]{1,0:T(8,128)(2,1)S(1)}, bf16[512,128]{1,0:T(8,128)(2,1)}, u32[]{:S(2)}) copy-start(bf16[512,128]{1,0:T(8,128)(2,1)} %param.19) | copy-start | bytes 393220
  27.0 5.1 %copy-start.9 = (f32[8]{0:T(128)S(1)}, f32[8]{0:T(128)}, u32[]{:S(2)}) copy-start(f32[8]{0:T(128)} %param.22) | copy-start | bytes 100
  35.4 2.5 %copy-start.7 = (bf16[512,2048]{1,0:T(8,128)(2,1)S(1)}, bf16[512,2048]{1,0:T(8,128)(2,1)}, u32[]{:S(2)}) copy-start(bf16[512,2048]{1,0:T(8,128)(2,1)} %param.23) | copy-start | bytes 6291460
  171.1 2.3 %copy-start.1 = (bf16[8,64,2048]{2,1,0:T(8,128)(2,1)S(1)}, bf16[8,64,2048]{2,1,0:T(8,128)(2,1)}, u32[]{:S(2)}) copy-start(bf16[8,64,2048]{2,1,0:T(8,128)(2,1)} %get-tuple-element.7) | copy-start | bytes 6291460
  171.1 4.7 %copy-start.3 = (bf16[128,2048]{1,0:T(8,128)(2,1)S(1)}, bf16[128,2048]{1,0:T(8,128)(2,1)}, u32[]{:S(2)}) copy-start(bf16[128,2048]{1,0:T(8,128)(2,1)} %get-tuple-element.36) | copy-start | bytes 1572868
